TPU v7x, 32 devices: a whole 2x2x4 slice. The times are simulated.
32 devices in a mesh: fs: 8 (over z, core), tp: 4 (over y, x).
Axes of the slice: x: 2, y: 2, z: 4, core: 2. Of those that a mesh axis runs over, the one named last changes fastest.
Arguments:
- gate_pre: bfloat16 [8192, 5632], P('fs', 'tp'), may hold values from -6 to 6
- up_pre: bfloat16 [8192, 5632], P('fs', 'tp'), may hold values from -6 to 6
- gate_taps: bfloat16 [3, 5632], replicated, may hold values from -3.5 to 3.5
- up_taps: bfloat16 [3, 5632], replicated, may hold values from -3.5 to 3.5
- down_proj: bfloat16 [5632, 2048], P('tp', 'fs'), may hold values from -0.078125 to 0.078125
- cotangent: bfloat16 [8192, 2048], P(('fs', 'tp')), may hold values from -6 to 6
Outputs:
- gate_grad: bfloat16 [8192, 5632], P('fs', 'tp')
- up_grad: bfloat16 [8192, 5632], P('fs', 'tp')
- down_grad: float32 [5632, 2048], P('tp', 'fs')
- row_norms: float32 [5632], P('tp')
- tap_grads: float32 [2, 3, 5632], replicated
All inputs are finite; a program needn't handle non-finite values.
Results may differ from a plain program's by a relative error of at most 0.0042.
Values may be sent and summed in bfloat16 or wider, within the bound.
No kernel may reach another device: no remote copies, remote signals or barrier semaphores. Data moves between devices by JAX's collectives and lax.ppermute only.
A program may use at most 128 MiB of HBM per device.

v0:
```python
import math
import jax
import jax.numpy as jnp
from jax import lax
from jax.sharding import PartitionSpec as P


def from_behind(block, axis, distance):
    devices = range(lax.axis_size(axis))
    route = [(i - distance, i) for i in devices if i - distance in devices]
    return lax.ppermute(block, axis, route)


def body(gate_pre, up_pre, gate_taps, up_taps, down_proj, cotangent):
    row_count = gate_pre.shape[0]
    channels = gate_pre.shape[1]
    tap_count = gate_taps.shape[0]
    reach = tap_count - 1
    channel_start = lax.axis_index("tp") * channels
    gate_taps_f = lax.dynamic_slice_in_dim(gate_taps, channel_start, channels, 1).astype(
        jnp.float32
    )
    up_taps_f = lax.dynamic_slice_in_dim(up_taps, channel_start, channels, 1).astype(jnp.float32)
    before = from_behind((gate_pre[row_count - reach :], up_pre[row_count - reach :]), "fs", 1)
    gate_padded = jnp.concatenate([before[0], gate_pre], axis=0).astype(jnp.float32)
    up_padded = jnp.concatenate([before[1], up_pre], axis=0).astype(jnp.float32)
    gate_conv = gate_taps_f[0] * gate_padded[0:row_count]
    up_conv = up_taps_f[0] * up_padded[0:row_count]
    for offset in range(1, tap_count):
        gate_conv = gate_conv + gate_taps_f[offset] * gate_padded[offset : offset + row_count]
        up_conv = up_conv + up_taps_f[offset] * up_padded[offset : offset + row_count]
    gate_sigmoid = jax.nn.sigmoid(gate_conv)
    gate_act = gate_conv * gate_sigmoid
    hidden = (gate_act * up_conv).astype(jnp.bfloat16)
    whole_cot = lax.all_gather(cotangent, "tp", axis=0, tiled=True)
    cot_cols = whole_cot
    hidden_grad = lax.dot_general(
        cot_cols,
        lax.all_gather(down_proj, "fs", axis=1, tiled=True),
        (((1,), (1,)), ((), ())),
        preferred_element_type=jnp.float32,
    )
    gate_conv_grad = hidden_grad * up_conv * gate_sigmoid * (1.0 + gate_conv * (1.0 - gate_sigmoid))
    up_conv_grad = hidden_grad * gate_act
    following = from_behind((gate_conv_grad[0:reach], up_conv_grad[0:reach]), "fs", -1)
    gate_grad_pad = jnp.concatenate([gate_conv_grad, following[0]], axis=0)
    up_grad_pad = jnp.concatenate([up_conv_grad, following[1]], axis=0)
    gate_grad = gate_taps_f[0] * gate_grad_pad[reach : reach + row_count]
    up_grad = up_taps_f[0] * up_grad_pad[reach : reach + row_count]
    for offset in range(1, tap_count):
        lead = reach - offset
        gate_grad = gate_grad + gate_taps_f[offset] * gate_grad_pad[lead : lead + row_count]
        up_grad = up_grad + up_taps_f[offset] * up_grad_pad[lead : lead + row_count]
    gate_tap_terms = jnp.stack(
        [
            jnp.sum(gate_conv_grad * gate_padded[offset : offset + row_count], axis=0)
            for offset in range(tap_count)
        ]
    )
    up_tap_terms = jnp.stack(
        [
            jnp.sum(up_conv_grad * up_padded[offset : offset + row_count], axis=0)
            for offset in range(tap_count)
        ]
    )
    tap_terms = jnp.stack([gate_tap_terms, up_tap_terms])
    feature_count = whole_cot.shape[1]
    grad_scale = 1.0 / math.sqrt(row_count * lax.axis_size("fs"))
    cot_cols = whole_cot
    own_rows = (
        lax.psum_scatter(
            lax.dot_general(
                cot_cols, hidden, (((0,), (0,)), ((), ())), preferred_element_type=jnp.float32
            ),
            "fs",
            scatter_dimension=0,
            tiled=True,
        )
        * grad_scale
    )
    down_grad = own_rows.T
    partial_norms = jnp.sum(own_rows * own_rows, axis=0)
    norm_sum, tap_sum = lax.psum((partial_norms, tap_terms), "fs")
    row_norms = norm_sum / feature_count
    tap_grads = lax.all_gather(tap_sum * grad_scale, "tp", axis=2, tiled=True)
    return (
        gate_grad.astype(jnp.bfloat16),
        up_grad.astype(jnp.bfloat16),
        down_grad,
        row_norms,
        tap_grads,
    )


def solution(mesh):
    placed = (P("fs", "tp"), P("fs", "tp"), P(), P(), P("tp", "fs"), P(("fs", "tp"), None))
    return jax.shard_map(
        body,
        mesh=mesh,
        in_specs=placed,
        out_specs=(P("fs", "tp"), P("fs", "tp"), P("tp", "fs"), P("tp"), P()),
        check_vma=False,
    )
```

profile of v0, /device:TPU:0, one launch (start us, length us, event | category | flops | bytes accessed | tf_op | source)
XLA Modules:
  0.0 337.2 jit_solution(16197569232840858787)
XLA Ops:
  7.2 0.0 copy-start
  7.2 0.0 all-gather.3.cloned.1.call-start
  7.2 0.7 all-gather.3.cloned.1.call-update
  7.9 0.0 all-gather.5.cloned.1.call-start
  8.0 0.7 all-gather.5.cloned.1.call-update
  8.7 0.0 reduce-scatter.2.cloned.1.call-start
  8.7 0.7 slice.74
  9.5 2.4 collective-permute-start
  11.9 0.7 slice.80
  12.6 4.6 %collective-permute-start.1 = (bf16[2,1408]{1,0:T(2,128)(2,1)S(1)}, bf16[2,1408]{1,0:T(2,128)(2,1)S(1)}, u32[]{:S(2)}, u32[]{:S(2)}) collective-permute-start(bf16[2,1408]{1,0:T(2,128)(2,1)S(1)} %slice.80), channel_id=1, source_target_pairs={{0,4},{4,8},{8,12},{12,16},{16,20},{20,24},{24,28},{1,5},{5,9},{9,... | collective-permute-start | bytes 16904 | tf_op jit(solution)/shard_map/ppermute | solution.py:11
  17.2 0.7 dynamic-slice_convert_fusion
  18.0 0.1 slice_reduce_fusion.5
  18.0 0.0 collective-permute-done
  18.1 5.2 %maximum_convert_fusion = f32[1026,1408]{1,0:T(8,128)} fusion(bf16[1024,1408]{1,0:T(8,128)(2,1)} %param.7, bf16[2,1408]{1,0:T(2,128)(2,1)S(1)} %collective-permute-done), kind=kLoop, calls=%fused_computation.31 | loop fusion | flops 5778432 | bytes 8667648 | tf_op jit(solution)/shard_map/convert_element_type | solution.py:26
  23.2 3.1 maximum_convert_fusion.1
  26.3 38.9 %all-gather.3.cloned.1.call-done = bf16[1024,2048]{1,0:T(8,128)(2,1)} async-done(((bf16[256,2048]{1,0:T(8,128)(2,1)}), bf16[1024,2048]{1,0:T(8,128)(2,1)}) %all-gather.3.cloned.1.call-update) | async-done | bytes 4194320 | tf_op jit(solution)/shard_map/all_gather | solution.py:35
  65.2 62.4 %all-gather.5.cloned.1.call-done = bf16[1408,2048]{1,0:T(8,128)(2,1)} async-done(((bf16[1408,256]{1,0:T(8,128)(2,1)}), bf16[1408,2048]{1,0:T(8,128)(2,1)}) %all-gather.5.cloned.1.call-update) | async-done | bytes 5767184 | tf_op jit(solution)/shard_map/all_gather | solution.py:39
  127.6 32.1 %multiply_reduce_fusion.5 = (f32[1408]{0:T(1024)S(1)}, f32[1408]{0:T(1024)S(1)}, f32[1408]{0:T(1024)S(1)}, f32[1024,1408]{1,0:T(8,128)}, f32[1024,1408]{1,0:T(8,...) fusion(f32[1026,1408]{1,0:T(8,128)} %maximum_convert_fusion.1, f32[1026,1408]{1,0:T(8,128)} %maximum_convert_fusion, ...), kind=kOutput, calls=%fused_computation.24 | convolution fusion | flops 5941620224 | bytes 67683840 | tf_op jit(solution)/shard_map/dot_general | solution.py:37
  159.7 14.2 %convolution_bitcast_fusion = f32[2048,1408]{0,1:T(8,128)} fusion(bf16[1024,2048]{1,0:T(8,128)(2,1)} %all-gather.3.cloned.1.call-done, f32[1024,1408]{1,0:T(8,128)} %get-tuple-element.25, f32[1024,1408]{1,0:T(8,128)} %get-tuple-element.26), kind=kOutput, calls=%fused_computation | convolution fusion | flops 5914230784 | bytes 27262976 | tf_op jit(solution)/shard_map/dot_general | solution.py:72
  173.8 0.0 reduce-scatter.2.cloned.1.call-update
  173.9 12.1 %multiply_reduce_fusion.2 = (f32[1408]{0:T(1024)S(1)}, f32[1408]{0:T(1024)S(1)}, f32[1408]{0:T(1024)S(1)}, f32[1024,1408]{1,0:T(8,128)S(1)}) fusion(f32[1026,1408]{1,0:T(8,128)} %maximum_convert_fusion, f32[1024,1408]{1,0:T(8,128)} %get-tuple-element.30, f32[1024,1408]{1,0:T(8,128)} %get-tuple-element.26), kind=kLoop, calls=%fused_computation.21 | loop fusion | flops 15855488 | bytes 34619904 | tf_op jit(solution)/shard_map/reduce_sum | solution.py:62
  186.2 1.3 collective-permute-start.2
  187.5 1.5 collective-permute-start.3
  189.0 0.2 collective-permute-done.2
  189.2 5.2 %fusion.9 = bf16[1024,1408]{1,0:T(8,128)(2,1)} fusion(f32[1024,1408]{1,0:T(8,128)S(1)} %bitcast.12, f32[2,1408]{1,0:T(2,128)S(1)} %collective-permute-done.2, f32[1408]{0:T(1024)S(1)} %get-tuple-element.20, f32[1408]{0:T(1024)S(1)} %get-tuple-element.21, f32[1408]{0:T(1024)S(1)} %get-tuple-element.19), kind=kLoop, calls=%fused_computation.14 | loop fusion | flops 11534336 | bytes 8678912 | tf_op jit(solution)/shard_map/convert_element_type | solution.py:87
  194.5 5.3 %fusion.4 = bf16[1024,1408]{1,0:T(8,128)(2,1)} fusion(f32[1024,1408]{1,0:T(8,128)S(1)} %get-tuple-element.27, f32[2,1408]{1,0:T(2,128)S(1)} %collective-permute-done.3, f32[1408]{0:T(1024)S(1)} %get-tuple-element.17, f32[1408]{0:T(1024)S(1)} %get-tuple-element.18, f32[1408]{0:T(1024)S(1)} %get-tuple-element.16), kind=kLoop, calls=%fused_computation.9 | loop fusion | flops 11534336 | bytes 8678912 | tf_op jit(solution)/shard_map/convert_element_type | solution.py:88
  199.8 91.9 %reduce-scatter.2.cloned.1.call-done = f32[256,1408]{0,1:T(8,128)} async-done(((f32[2048,1408]{0,1:T(8,128)}), f32[256,1408]{0,1:T(8,128)}) %reduce-scatter.2.cloned.1.call-update) | async-done | bytes 1441808 | tf_op jit(solution)/shard_map/reduce_scatter | solution.py:71
  291.7 2.6 multiply_reduce_fusion.6
  294.3 26.4 %all-reduce = (f32[1408]{0:T(1024)S(1)}, f32[2,3,1408]{2,1,0:T(4,128)S(1)}) all-reduce(f32[1408]{0:T(1024)S(1)} %get-tuple-element.28, f32[2,3,1408]{2,1,0:T(4,128)S(1)} %pad_maximum_fusion.2), channel_id=1, replica_groups=mesh['fs'=8,'tp'=4] {'fs'}, use_global_device_ids=true, to_apply=%region_2.0 | all-reduce | flops 9856 | bytes 78848 | tf_op jit(solution)/shard_map/psum | solution.py:83
  320.6 0.6 broadcast_multiply_fusion.1
  321.2 8.7 %all_gather.11 = f32[2,3,5632]{2,1,0:T(4,128)S(1)} all-gather(f32[2,3,1408]{2,1,0:T(4,128)S(1)} %broadcast_multiply_fusion), channel_id=1, replica_groups=mesh['fs'=8,'tp'=4] {'tp'}, dimensions={2}, use_global_device_ids=true | all-gather | bytes 168960 | tf_op jit(solution)/shard_map/all_gather | solution.py:85
  329.9 0.7 copy.11
  (21 shorter events, 0.2 us)
Async XLA Ops:
  7.2 16.1 %copy-start = (bf16[1024,1408]{1,0:T(8,128)(2,1)S(1)}, bf16[1024,1408]{1,0:T(8,128)(2,1)}, u32[]{:S(2)}) copy-start(bf16[1024,1408]{1,0:T(8,128)(2,1)} %param.6) | copy-start | bytes 8650756
  7.2 58.0 %all-gather.3.cloned.1.call-start = ((), (), s32[]{:S(2)}) async-start(), calls=%async_computation.1 | async-start | bytes 5242880 | tf_op jit(solution)/shard_map/all_gather | solution.py:35
  7.9 119.7 %all-gather.5.cloned.1.call-start = ((), (), s32[]{:S(2)}) async-start(), calls=%async_computation.2 | async-start | bytes 6488064 | tf_op jit(solution)/shard_map/all_gather | solution.py:39
  8.7 283.0 %reduce-scatter.2.cloned.1.call-start = ((), (), s32[]{:S(2)}) async-start(), calls=%async_computation.3 | async-start | bytes 12976128 | tf_op jit(solution)/shard_map/reduce_scatter | solution.py:71
  9.5 8.6 %collective-permute-start = (bf16[2,1408]{1,0:T(2,128)(2,1)S(1)}, bf16[2,1408]{1,0:T(2,128)(2,1)S(1)}, u32[]{:S(2)}, u32[]{:S(2)}) collective-permute-start(bf16[2,1408]{1,0:T(2,128)(2,1)S(1)} %slice.74), channel_id=1, source_target_pairs={{0,4},{4,8},{8,12},{12,16},{16,20},{20,24},{24,28},{1,5},{5,9},{9,... | collective-permute-start | bytes 16904 | tf_op jit(solution)/shard_map/ppermute | solution.py:11
  12.6 10.6 %collective-permute-start.1 = (bf16[2,1408]{1,0:T(2,128)(2,1)S(1)}, bf16[2,1408]{1,0:T(2,128)(2,1)S(1)}, u32[]{:S(2)}, u32[]{:S(2)}) collective-permute-start(bf16[2,1408]{1,0:T(2,128)(2,1)S(1)} %slice.80), channel_id=1, source_target_pairs={{0,4},{4,8},{8,12},{12,16},{16,20},{20,24},{24,28},{1,5},{5,9},{9,... | collective-permute-start | bytes 16904 | tf_op jit(solution)/shard_map/ppermute | solution.py:11
  173.8 12.3 %slice-start = ((s8[5767168]{0:T(1024)(128)(4,1)}), s8[1572864]{0:T(1024)(128)(4,1)S(1)}, s32[]{:S(2)}) async-start(s8[5767168]{0:T(1024)(128)(4,1)} %bitcast.11), calls=%async_computation.4 | async-start | bytes 3145728
  173.9 12.3 %slice-start.1 = ((s8[5767168]{0:T(1024)(128)(4,1)}), s8[4194304]{0:T(1024)(128)(4,1)S(1)}, s32[]{:S(2)}) async-start(s8[5767168]{0:T(1024)(128)(4,1)} %bitcast.11), calls=%async_computation.5 | async-start | bytes 8388608
  186.2 3.1 collective-permute-start.2
  187.5 7.0 %collective-permute-start.3 = (f32[2,1408]{1,0:T(2,128)S(1)}, f32[2,1408]{1,0:T(2,128)S(1)}, u32[]{:S(2)}, u32[]{:S(2)}) collective-permute-start(f32[2,1408]{1,0:T(2,128)S(1)} %slice.107), channel_id=1, source_target_pairs={{4,0},{8,4},{12,8},{16,12},{20,16},{24,20},{28,24},{5,1},{9,5},{13... | collective-permute-start | bytes 33800 | tf_op jit(solution)/shard_map/ppermute | solution.py:11
Sparse Core Ops, SparseCore 0:
  9.8 55.2 all-gather.2
  66.7 60.7 all-gather.4
  174.0 117.6 reduce-scatter.1
where the time goes:
time: 338 us; the launch traced here: 337 us
  waiting for transfers between devices  195 us (58%)
  matrix products  46.2 us (14%)
  blocking collectives  35 us (10%)
  other arithmetic  34.9 us (10%)
  between operations  14 us (4%)
  starting transfers between devices  9.86 us (3%)
    reduce_scatter x1, waiting for transfers between devices, body(): lax.psum_scatter(lax.dot_general(cot_cols, hidden, (((0,), (0,)), ((), ()...  91.9 us
    all_gather x1, waiting for transfers between devices, body(): lax.all_gather(down_proj, 'fs', axis=1, tiled=True)  62.4 us
    all_gather x1, waiting for transfers between devices, body(): whole_cot = lax.all_gather(cotangent, 'tp', axis=0, tiled=True)  38.9 us
    dot_general x1, matrix products, body(): lax.dot_general(cot_cols, lax.all_gather(down_proj, 'fs', axis=1, tiled=T...  32.1 us
    psum x1, blocking collectives, body(): norm_sum, tap_sum = lax.psum((partial_norms, tap_terms), 'fs')  26.4 us
    dot_general x1, matrix products, body(): lax.dot_general(cot_cols, hidden, (((0,), (0,)), ((), ())), preferred_ele...  14.2 us
    reduce_sum x1, other arithmetic, body(): jnp.sum(up_conv_grad * up_padded[offset:offset + row_count], axis=0)  12.1 us
    ppermute x4, starting transfers between devices, from_behind(): return lax.ppermute(block, axis, route)  9.74 us
  transfers between devices with their start and end apart: 7, of which 4 were waited for; matrix products, arithmetic and copies ran while one was open for 10% of the time, Pallas kernels for 0%

commit v1 on v0

--- a/solution.py
+++ b/solution.py
@@ -32,7 +32,12 @@
     gate_sigmoid = jax.nn.sigmoid(gate_conv)
     gate_act = gate_conv * gate_sigmoid
     hidden = (gate_act * up_conv).astype(jnp.bfloat16)
-    whole_cot = lax.all_gather(cotangent, "tp", axis=0, tiled=True)
+    ring = [cotangent]
+    for hop in range(3):
+        ring.append(lax.ppermute(ring[-1], "tp", [(dev, (dev + 1) % 4) for dev in range(4)]))
+    whole_cot = jnp.roll(
+        jnp.concatenate(ring[::-1], axis=0), (lax.axis_index("tp") + 1) * ring[0].shape[0], axis=0
+    )
     cot_cols = whole_cot
     hidden_grad = lax.dot_general(
         cot_cols,

time: 338 us -> 306 us (0.905)
  waiting for transfers between devices: 195 us -> 152 us
  local copies, waits for them, and re-layouts: 2.38 us -> 12.5 us
    all_gather x1, waiting for transfers between devices: 62.4 us -> 0.01 us  [body(): lax.all_gather(down_proj, 'fs', axis=1, tiled=True)]
    ppermute x0 -> x3, waiting for transfers between devices: none -> 57.5 us  [body(): lax.ppermute(ring[-1], 'tp', [(dev, (dev + 1) % 4) for dev in range(4)])]
    all_gather x1 -> x0, waiting for transfers between devices: 38.9 us -> none  [body(): whole_cot = lax.all_gather(cotangent, 'tp', axis=0, tiled=True)]
    unnamed x7 -> x17, local copies, waits for them, and re-layouts: 0.74 us -> 9.78 us
    ppermute x0 -> x3, starting transfers between devices: none -> 3.8 us  [body(): lax.ppermute(ring[-1], 'tp', [(dev, (dev + 1) % 4) for dev in range(4)])]
  transfers between devices with their start and end apart: 7 -> 9, of which waited for: 4 -> 5; matrix products, arithmetic and copies ran while one was open for 10% -> 14% of each run, Pallas kernels for 0% -> 0%
where the time goes in v1:
time: 306 us; the launch traced here: 305 us
  waiting for transfers between devices  152 us (50%)
  matrix products  45.7 us (15%)
  blocking collectives  35.1 us (11%)
  other arithmetic  33.5 us (11%)
  between operations  14.3 us (5%)
  local copies, waits for them, and re-layouts  12.5 us (4%)
  starting transfers between devices  12.1 us (4%)
    reduce_scatter x1, waiting for transfers between devices, body(): lax.psum_scatter(lax.dot_general(cot_cols, hidden, (((0,), (0,)), ((), ()...  93.8 us
    ppermute x3, waiting for transfers between devices, body(): lax.ppermute(ring[-1], 'tp', [(dev, (dev + 1) % 4) for dev in range(4)])  57.5 us
    dot_general x1, matrix products, body(): lax.dot_general(cot_cols, lax.all_gather(down_proj, 'fs', axis=1, tiled=T...  31 us
    psum x1, blocking collectives, body(): norm_sum, tap_sum = lax.psum((partial_norms, tap_terms), 'fs')  26.4 us
    dot_general x1, matrix products, body(): lax.dot_general(cot_cols, hidden, (((0,), (0,)), ((), ())), preferred_ele...  14.6 us
    reduce_sum x1, other arithmetic, body(): jnp.sum(up_conv_grad * up_padded[offset:offset + row_count], axis=0)  12.1 us
    unnamed x17, local copies, waits for them, and re-layouts  9.78 us
    all_gather x1, blocking collectives, body(): tap_grads = lax.all_gather(tap_sum * grad_scale, 'tp', axis=2, tiled=True)  8.7 us
  transfers between devices with their start and end apart: 9, of which 5 were waited for; matrix products, arithmetic and copies ran while one was open for 14% of the time, Pallas kernels for 0%

profile of v1, /device:TPU:0, one launch (start us, length us, event | category | flops | bytes accessed | tf_op | source)
XLA Modules:
  0.0 305.4 jit_solution(15671896787286628230)
XLA Ops:
  7.9 3.0 collective-permute-start
  11.0 24.3 %collective-permute-done = bf16[256,2048]{1,0:T(8,128)(2,1)S(1)} collective-permute-done((bf16[256,2048]{1,0:T(8,128)(2,1)}, bf16[256,2048]{1,0:T(8,128)(2,1)S(1)}, u32[]{:S(2)}, u32[]{:S(2)}) %collective-permute-start) | collective-permute-done | bytes 1048608 | tf_op jit(solution)/shard_map/ppermute | solution.py:37
  35.3 0.8 collective-permute-start.1
  36.1 0.7 slice.74
  36.8 1.3 collective-permute-start.3
  38.1 0.7 slice.80
  38.9 4.2 %collective-permute-start.4 = (bf16[2,1408]{1,0:T(2,128)(2,1)S(1)}, bf16[2,1408]{1,0:T(2,128)(2,1)S(1)}, u32[]{:S(2)}, u32[]{:S(2)}) collective-permute-start(bf16[2,1408]{1,0:T(2,128)(2,1)S(1)} %slice.80), channel_id=1, source_target_pairs={{0,4},{4,8},{8,12},{12,16},{16,20},{20,24},{24,28},{1,5},{5,9},{9,... | collective-permute-start | bytes 16904 | tf_op jit(solution)/shard_map/ppermute | solution.py:11
  43.1 0.7 dynamic-slice_convert_fusion
  44.0 16.7 %collective-permute-done.1 = bf16[256,2048]{1,0:T(8,128)(2,1)S(1)} collective-permute-done((bf16[256,2048]{1,0:T(8,128)(2,1)S(1)}, bf16[256,2048]{1,0:T(8,128)(2,1)S(1)}, u32[]{:S(2)}, u32[]{:S(2)}) %collective-permute-start.1) | collective-permute-done | bytes 1048608 | tf_op jit(solution)/shard_map/ppermute | solution.py:37
  60.6 4.9 %maximum_convert_fusion = f32[1026,1408]{1,0:T(8,128)} fusion(bf16[1024,1408]{1,0:T(8,128)(2,1)} %param.7, bf16[2,1408]{1,0:T(2,128)(2,1)S(1)} %collective-permute-done.3), kind=kLoop, calls=%fused_computation.34 | loop fusion | flops 5778432 | bytes 8667648 | tf_op jit(solution)/shard_map/convert_element_type | solution.py:26
  65.5 3.1 %maximum_convert_fusion.1 = f32[1026,1408]{1,0:T(8,128)} fusion(bf16[1024,1408]{1,0:T(8,128)(2,1)S(1)} %copy-done.1, bf16[2,1408]{1,0:T(2,128)(2,1)S(1)} %collective-permute-done.4), kind=kLoop, calls=%fused_computation.35 | loop fusion | flops 5778432 | bytes 8667648 | tf_op jit(solution)/shard_map/convert_element_type | solution.py:25
  68.6 16.5 %collective-permute-done.2 = bf16[256,2048]{1,0:T(8,128)(2,1)S(1)} collective-permute-done((bf16[256,2048]{1,0:T(8,128)(2,1)S(1)}, bf16[256,2048]{1,0:T(8,128)(2,1)S(1)}, u32[]{:S(2)}, u32[]{:S(2)}) %collective-permute-start.2) | collective-permute-done | bytes 1048608 | tf_op jit(solution)/shard_map/ppermute | solution.py:37
  85.1 1.1 constant_dynamic-update-slice_fusion.7
  86.2 1.0 constant_dynamic-update-slice_fusion.6
  87.2 1.1 constant_dynamic-update-slice_fusion.5
  88.3 1.1 constant_dynamic-update-slice_fusion.4
  89.4 1.1 constant_dynamic-update-slice_fusion.3
  90.5 1.0 constant_dynamic-update-slice_fusion.2
  91.5 1.1 constant_dynamic-update-slice_fusion.1
  92.6 1.1 constant_dynamic-update-slice_fusion
  93.7 31.0 %multiply_reduce_fusion.5 = (f32[1408]{0:T(1024)S(1)}, f32[1408]{0:T(1024)S(1)}, f32[1408]{0:T(1024)S(1)}, f32[1024,1408]{1,0:T(8,128)}, f32[1024,1408]{1,0:T(8,...) fusion(f32[1026,1408]{1,0:T(8,128)} %maximum_convert_fusion.1, f32[1026,1408]{1,0:T(8,128)} %maximum_convert_fusion, ...), kind=kOutput, calls=%fused_computation.23 | convolution fusion | flops 5941620224 | bytes 67683840 | tf_op jit(solution)/shard_map/dot_general | solution.py:42
  124.7 14.6 %fusion.13 = f32[2048,1408]{1,0:T(8,128)} fusion(bf16[2048,2048]{1,0:T(8,128)(2,1)} %constant_dynamic-update-slice_fusion, s32[]{:T(128)S(6)} %select_n.19, f32[1024,1408]{1,0:T(8,128)} %get-tuple-element.30, f32[1024,1408]{1,0:T(8,128)} %get-tuple-element.31), kind=kOutput, calls=%fused_computation.30 | convolution fusion | flops 5914230784 | bytes 27262980 | tf_op jit(solution)/shard_map/dot_general | solution.py:77
  139.4 12.1 %multiply_reduce_fusion.2 = (f32[1408]{0:T(1024)S(1)}, f32[1408]{0:T(1024)S(1)}, f32[1408]{0:T(1024)S(1)}, f32[1024,1408]{1,0:T(8,128)S(1)}) fusion(f32[1026,1408]{1,0:T(8,128)} %maximum_convert_fusion, f32[1024,1408]{1,0:T(8,128)} %get-tuple-element.35, f32[1024,1408]{1,0:T(8,128)} %get-tuple-element.31), kind=kLoop, calls=%fused_computation.20 | loop fusion | flops 15855488 | bytes 34619904 | tf_op jit(solution)/shard_map/reduce_sum | solution.py:67
  151.6 1.3 collective-permute-start.5
  152.9 1.5 collective-permute-start.6
  154.7 5.2 %fusion.9 = bf16[1024,1408]{1,0:T(8,128)(2,1)} fusion(f32[1024,1408]{1,0:T(8,128)S(1)} %bitcast.8, f32[2,1408]{1,0:T(2,128)S(1)} %collective-permute-done.5, f32[1408]{0:T(1024)S(1)} %get-tuple-element.25, f32[1408]{0:T(1024)S(1)} %get-tuple-element.26, f32[1408]{0:T(1024)S(1)} %get-tuple-element.24), kind=kLoop, calls=%fused_computation.13 | loop fusion | flops 11534336 | bytes 8678912 | tf_op jit(solution)/shard_map/convert_element_type | solution.py:92
  159.9 5.3 %fusion.4 = bf16[1024,1408]{1,0:T(8,128)(2,1)} fusion(f32[1024,1408]{1,0:T(8,128)S(1)} %get-tuple-element.32, f32[2,1408]{1,0:T(2,128)S(1)} %collective-permute-done.6, f32[1408]{0:T(1024)S(1)} %get-tuple-element.22, f32[1408]{0:T(1024)S(1)} %get-tuple-element.23, f32[1408]{0:T(1024)S(1)} %get-tuple-element.21), kind=kLoop, calls=%fused_computation.8 | loop fusion | flops 11534336 | bytes 8678912 | tf_op jit(solution)/shard_map/convert_element_type | solution.py:93
  165.2 93.8 %reduce-scatter.2.cloned.1.call-done = f32[256,1408]{1,0:T(8,128)} async-done(((f32[2048,1408]{1,0:T(8,128)}), f32[256,1408]{1,0:T(8,128)}) %reduce-scatter.2.cloned.1.call-update) | async-done | bytes 1441808 | tf_op jit(solution)/shard_map/reduce_scatter | solution.py:76
  259.0 1.5 multiply_reduce_fusion.6
  260.6 26.4 %all-reduce = (f32[1408]{0:T(1024)S(1)}, f32[2,3,1408]{2,1,0:T(4,128)S(1)}) all-reduce(f32[1408]{0:T(1024)S(1)} %get-tuple-element.33, f32[2,3,1408]{2,1,0:T(4,128)S(1)} %pad_maximum_fusion.2), channel_id=1, replica_groups=mesh['fs'=8,'tp'=4] {'fs'}, use_global_device_ids=true, to_apply=%region_2.3 | all-reduce | flops 9856 | bytes 78848 | tf_op jit(solution)/shard_map/psum | solution.py:88
  287.6 8.7 %all_gather.7 = f32[2,3,5632]{2,1,0:T(4,128)S(1)} all-gather(f32[2,3,1408]{2,1,0:T(4,128)S(1)} %broadcast_multiply_fusion), channel_id=1, replica_groups=mesh['fs'=8,'tp'=4] {'tp'}, dimensions={2}, use_global_device_ids=true | all-gather | bytes 168960 | tf_op jit(solution)/shard_map/all_gather | solution.py:90
  297.0 1.5 copy.12
  (35 shorter events, 2.6 us)
Async XLA Ops:
  7.2 86.5 %all-gather.2.cloned.1.call-start = ((), (), s32[]{:S(2)}) async-start(), calls=%async_computation.1 | async-start | bytes 6488064 | tf_op jit(solution)/shard_map/all_gather | solution.py:44
  7.9 251.1 %reduce-scatter.2.cloned.1.call-start = ((), (), s32[]{:S(2)}) async-start(), calls=%async_computation.2 | async-start | bytes 12976128 | tf_op jit(solution)/shard_map/reduce_scatter | solution.py:76
  7.9 27.3 %collective-permute-start = (bf16[256,2048]{1,0:T(8,128)(2,1)}, bf16[256,2048]{1,0:T(8,128)(2,1)S(1)}, u32[]{:S(2)}, u32[]{:S(2)}) collective-permute-start(bf16[256,2048]{1,0:T(8,128)(2,1)} %param.11), channel_id=1, source_target_pairs={{0,1},{1,2},{2,3},{3,0},{4,5},{5,6},{6,7},{7,4},{8,9},{9,10},{10,1... | collective-permute-start | bytes 3145736 | tf_op jit(solution)/shard_map/ppermute | solution.py:37
  35.3 25.3 %collective-permute-start.1 = (bf16[256,2048]{1,0:T(8,128)(2,1)S(1)}, bf16[256,2048]{1,0:T(8,128)(2,1)S(1)}, u32[]{:S(2)}, u32[]{:S(2)}) collective-permute-start(bf16[256,2048]{1,0:T(8,128)(2,1)S(1)} %collective-permute-done), channel_id=1, source_target_pairs={{0,1},{1,2},{2,3},{3,0},{4,5},{5,6},{6,7},{7,4},{8,9},{9,10},{10,1... | collective-permute-start | bytes 3145736 | tf_op jit(solution)/shard_map/ppermute | solution.py:37
  36.8 23.8 %collective-permute-start.3 = (bf16[2,1408]{1,0:T(2,128)(2,1)S(1)}, bf16[2,1408]{1,0:T(2,128)(2,1)S(1)}, u32[]{:S(2)}, u32[]{:S(2)}) collective-permute-start(bf16[2,1408]{1,0:T(2,128)(2,1)S(1)} %slice.74), channel_id=1, source_target_pairs={{0,4},{4,8},{8,12},{12,16},{16,20},{20,24},{24,28},{1,5},{5,9},{9,... | collective-permute-start | bytes 16904 | tf_op jit(solution)/shard_map/ppermute | solution.py:11
  38.9 26.6 %collective-permute-start.4 = (bf16[2,1408]{1,0:T(2,128)(2,1)S(1)}, bf16[2,1408]{1,0:T(2,128)(2,1)S(1)}, u32[]{:S(2)}, u32[]{:S(2)}) collective-permute-start(bf16[2,1408]{1,0:T(2,128)(2,1)S(1)} %slice.80), channel_id=1, source_target_pairs={{0,4},{4,8},{8,12},{12,16},{16,20},{20,24},{24,28},{1,5},{5,9},{9,... | collective-permute-start | bytes 16904 | tf_op jit(solution)/shard_map/ppermute | solution.py:11
  43.9 21.6 %copy-start.1 = (bf16[1024,1408]{1,0:T(8,128)(2,1)S(1)}, bf16[1024,1408]{1,0:T(8,128)(2,1)}, u32[]{:S(2)}) copy-start(bf16[1024,1408]{1,0:T(8,128)(2,1)} %param.6) | copy-start | bytes 8650756
  60.6 24.5 %collective-permute-start.2 = (bf16[256,2048]{1,0:T(8,128)(2,1)S(1)}, bf16[256,2048]{1,0:T(8,128)(2,1)S(1)}, u32[]{:S(2)}, u32[]{:S(2)}) collective-permute-start(bf16[256,2048]{1,0:T(8,128)(2,1)S(1)} %collective-permute-done.1), channel_id=1, source_target_pairs={{0,1},{1,2},{2,3},{3,0},{4,5},{5,6},{6,7},{7,4},{8,9},{9,10},{10,1... | collective-permute-start | bytes 3145736 | tf_op jit(solution)/shard_map/ppermute | solution.py:37
  65.5 22.8 %copy-start = (bf16[256,2048]{1,0:T(8,128)(2,1)S(1)}, bf16[256,2048]{1,0:T(8,128)(2,1)}, u32[]{:S(2)}) copy-start(bf16[256,2048]{1,0:T(8,128)(2,1)} %param.11) | copy-start | bytes 3145732
  139.3 12.2 %slice-start = ((s8[5767168]{0:T(1024)(128)(4,1)}), s8[1572864]{0:T(1024)(128)(4,1)S(1)}, s32[]{:S(2)}) async-start(s8[5767168]{0:T(1024)(128)(4,1)} %bitcast.7), calls=%async_computation.3 | async-start | bytes 3145728
  139.3 12.2 %slice-start.1 = ((s8[5767168]{0:T(1024)(128)(4,1)}), s8[4194304]{0:T(1024)(128)(4,1)S(1)}, s32[]{:S(2)}) async-start(s8[5767168]{0:T(1024)(128)(4,1)} %bitcast.7), calls=%async_computation.4 | async-start | bytes 8388608
  151.6 3.1 %collective-permute-start.5 = (f32[2,1408]{1,0:T(2,128)S(1)}, f32[2,1408]{1,0:T(2,128)S(1)}, u32[]{:S(2)}, u32[]{:S(2)}) collective-permute-start(f32[2,1408]{1,0:T(2,128)S(1)} %slice.104), channel_id=1, source_target_pairs={{4,0},{8,4},{12,8},{16,12},{20,16},{24,20},{28,24},{5,1},{9,5},{13... | collective-permute-start | bytes 33800 | tf_op jit(solution)/shard_map/ppermute | solution.py:11
  152.9 7.0 %collective-permute-start.6 = (f32[2,1408]{1,0:T(2,128)S(1)}, f32[2,1408]{1,0:T(2,128)S(1)}, u32[]{:S(2)}, u32[]{:S(2)}) collective-permute-start(f32[2,1408]{1,0:T(2,128)S(1)} %slice.107), channel_id=1, source_target_pairs={{4,0},{8,4},{12,8},{16,12},{20,16},{24,20},{28,24},{5,1},{9,5},{13... | collective-permute-start | bytes 33800 | tf_op jit(solution)/shard_map/ppermute | solution.py:11
Sparse Core Ops, SparseCore 0:
  9.6 63.5 all-gather.1
  139.5 119.5 reduce-scatter.1
